TPU v7x, 32 devices: a whole 2x2x4 slice. The times are simulated.
32 devices in a mesh: rep: 2 (over x), fs: 8 (over z, y), tp: 2 (over core).
Axes of the slice: x: 2, y: 2, z: 4, core: 2. Of those that a mesh axis runs over, the one named last changes fastest.
Arguments:
- tokens: bfloat16 [4096, 1024], P(('rep', 'fs', 'tp')), may hold values from -4 to 4
- mixer_out: bfloat16 [4096, 1024], P(('rep', 'fs')), may hold values from -4 to 4
- gain_first: float32 [1024], replicated, may hold values from 0.1 to 1.9
- gate_first: bfloat16 [1024, 2816], P('fs', 'tp'), may hold values from -0.1875 to 0.1875
- up_first: bfloat16 [1024, 2816], P('fs', 'tp'), may hold values from -0.1875 to 0.1875
- down_first: bfloat16 [2816, 1024], P('tp', 'fs'), may hold values from -0.109375 to 0.109375
- gain_second: float32 [1024], replicated, may hold values from 0.1 to 1.9
- gate_second: bfloat16 [1024, 2816], P('fs', 'tp'), may hold values from -0.1875 to 0.1875
- up_second: bfloat16 [1024, 2816], P('fs', 'tp'), may hold values from -0.1875 to 0.1875
- down_second: bfloat16 [2816, 1024], P('tp', 'fs'), may hold values from -0.109375 to 0.109375
- gain_last: float32 [1024], P('tp'), may hold values from 0.1 to 1.9
Outputs:
- result: bfloat16 [4096, 1024], P(('rep', 'fs'), 'tp')
All inputs are finite; a program needn't handle non-finite values.
Results may differ from a plain program's by a relative error of at most 0.02.
Values may be sent and summed in bfloat16 or wider, within the bound.
A program may use at most 64 MiB of HBM per device.

v0:
```python
import jax
import jax.numpy as jnp
from jax import lax
from jax.sharding import PartitionSpec as P

EPS = 1e-06


def over_all(slab, axis, dim):

    def gathered(part):
        return lax.all_gather(part, axis, axis=dim, tiled=True)

    return jax.tree.map(gathered, slab)


def normalize(floats_in, gain_vec):
    floats = floats_in.astype(jnp.float32)
    factor = lax.rsqrt(jnp.mean(floats * floats, axis=-1, keepdims=True) + EPS)
    return (floats * factor * gain_vec.astype(jnp.float32)).astype(jnp.bfloat16)


def gather_group(row_block):
    return lax.all_gather(row_block, "tp", axis=0, tiled=True)


def inner_hidden(normed, w_gate, w_up):

    def add_both(totals, pieces):
        columns = lax.slice_in_dim(normed, 0, pieces[0].shape[0], axis=1)
        return (
            totals[0] + jnp.dot(columns, pieces[0], preferred_element_type=jnp.float32),
            totals[1] + jnp.dot(columns, pieces[1], preferred_element_type=jnp.float32),
        )

    empty = jnp.zeros((normed.shape[0], w_gate.shape[1]), jnp.float32)
    gate_acc, up_acc = add_both((empty, empty), over_all((w_gate, w_up), "fs", 0))
    return (jax.nn.silu(gate_acc) * up_acc).astype(jnp.bfloat16)


def outer_weight(w_down):
    return lax.all_gather(w_down, "fs", axis=1, tiled=True)


def local(
    tokens,
    mixer_out,
    gain_first,
    gate_first,
    up_first,
    down_first,
    gain_second,
    gate_second,
    up_second,
    down_second,
    gain_last,
):
    rows_dev = tokens.shape[0]
    tp_count = lax.axis_size("tp")
    tp_index = lax.axis_index("tp")
    normed_own = normalize(tokens, gain_first)
    normed_one = gather_group(normed_own)
    hidden_one = inner_hidden(normed_one, gate_first, up_first)
    down_full = outer_weight(down_first)

    def row_terms():
        picked = lax.slice_in_dim(hidden_one, 0, rows_dev * lax.axis_size("tp"), axis=0)
        return jnp.dot(picked, down_full, preferred_element_type=jnp.float32)

    ffn_one = lax.psum_scatter(
        row_terms().astype(jnp.bfloat16), "tp", scatter_dimension=0, tiled=True
    ).astype(jnp.float32)
    after_one = (tokens.astype(jnp.float32) + 0.5 * ffn_one).astype(jnp.bfloat16)
    own_mixer = lax.dynamic_slice_in_dim(mixer_out, tp_index * rows_dev, rows_dev, 0)
    mixed_in = (after_one.astype(jnp.float32) + own_mixer.astype(jnp.float32)).astype(jnp.bfloat16)
    gathered = gather_group(mixed_in)
    normed_two = normalize(gathered, gain_second)
    hidden_two = inner_hidden(normed_two, gate_second, up_second)
    down_two_full = outer_weight(down_second)
    terms_two = jnp.dot(hidden_two, down_two_full, preferred_element_type=jnp.float32)
    ffn_two = lax.psum_scatter(
        terms_two.astype(jnp.bfloat16), "tp", scatter_dimension=1, tiled=True
    ).astype(jnp.float32)
    col_width = ffn_two.shape[1]
    my_cols = lax.dynamic_slice_in_dim(gathered, tp_index * col_width, col_width, 1)
    after_two = (my_cols.astype(jnp.float32) + 0.5 * ffn_two).astype(jnp.bfloat16)
    floats = after_two.astype(jnp.float32)
    sum_sq = lax.psum(jnp.sum(floats * floats, axis=1), "tp")
    factor = lax.rsqrt(sum_sq / (col_width * tp_count) + EPS)
    return (floats * factor[:, None] * gain_last.astype(jnp.float32)[None, :]).astype(jnp.bfloat16)


def solution(mesh):
    in_specs = (
        P(("rep", "fs", "tp"), None),
        P(("rep", "fs"), None),
        P(),
        P("fs", "tp"),
        P("fs", "tp"),
        P("tp", "fs"),
        P(),
        P("fs", "tp"),
        P("fs", "tp"),
        P("tp", "fs"),
        P("tp"),
    )
    out_specs = P(("rep", "fs"), "tp")
    return jax.shard_map(local, mesh=mesh, in_specs=in_specs, out_specs=out_specs, check_vma=False)
```

profile of v0, /device:TPU:0, one launch (start us, length us, event | category | flops | bytes accessed | tf_op | source)
XLA Modules:
  0.0 402.3 jit_solution(16282262251810732455)
XLA Ops:
  6.5 0.7 all-gather.7.cloned.1.call-update
  7.3 0.7 all-gather.11.cloned.1.call-update
  8.1 0.7 all-gather.9.cloned.1.call-update
  8.8 1.1 fusion.10
  9.9 1.1 fusion.12
  11.0 2.3 all_gather.24
  13.3 56.3 %all-gather.7.cloned.1.call-done = bf16[1024,1408]{1,0:T(8,128)(2,1)} async-done(((bf16[128,1408]{1,0:T(8,128)(2,1)}), bf16[1024,1408]{1,0:T(8,128)(2,1)}) %all-gather.7.cloned.1.call-update) | async-done | bytes 2883600 | tf_op jit(solution)/shard_map/all_gather | solution.py:12
  69.6 2.8 fusion.20
  72.4 57.4 %all-gather.11.cloned.1.call-done = bf16[1408,1024]{1,0:T(8,128)(2,1)} async-done(((bf16[1408,128]{1,0:T(8,128)(2,1)}), bf16[1408,1024]{1,0:T(8,128)(2,1)}) %all-gather.11.cloned.1.call-update) | async-done | bytes 2883600 | tf_op jit(solution)/shard_map/all_gather | solution.py:42
  129.8 57.7 %all-gather.9.cloned.1.call-done = bf16[1024,1408]{1,0:T(8,128)(2,1)} async-done(((bf16[128,1408]{1,0:T(8,128)(2,1)}), bf16[1024,1408]{1,0:T(8,128)(2,1)}) %all-gather.9.cloned.1.call-update) | async-done | bytes 2883600 | tf_op jit(solution)/shard_map/all_gather | solution.py:12
  187.5 5.4 %convolution_convert_fusion.1 = bf16[256,1024]{1,0:T(8,128)(2,1)} fusion(bf16[1408,1024]{1,0:T(8,128)(2,1)} %all-gather.11.cloned.1.call-done, bf16[256,1024]{1,0:T(8,128)(2,1)S(1)} %all_gather.24, bf16[1024,1408]{1,0:T(8,128)(2,1)} %all-gather.9.cloned.1.call-done, f32[256,1408]{1,0:T(8,128)S(1)} %fusion.20), kind=kOutput, calls=%fused_computation.7 | convolution fusion | flops 1478819840 | bytes 8257536 | tf_op jit(solution)/shard_map/dot_general | solution.py:68
  194.2 0.7 all-gather.17.cloned.1.call-update
  194.9 4.7 %reduce-scatter.3.cloned.1.call-done = bf16[128,1024]{1,0:T(8,128)(2,1)} async-done(((bf16[256,1024]{1,0:T(8,128)(2,1)}), bf16[128,1024]{1,0:T(8,128)(2,1)}) %reduce-scatter.3.cloned.1.call-update) | async-done | bytes 262160 | tf_op jit(solution)/shard_map/reduce_scatter | solution.py:70
  199.7 1.1 add_convert_fusion.1
  200.7 2.2 all_gather.28
  203.1 57.0 %all-gather.13.cloned.1.call-done = bf16[1024,1408]{1,0:T(8,128)(2,1)} async-done(((bf16[128,1408]{1,0:T(8,128)(2,1)}), bf16[1024,1408]{1,0:T(8,128)(2,1)}) %all-gather.13.cloned.1.call-update) | async-done | bytes 2883600 | tf_op jit(solution)/shard_map/all_gather | solution.py:12
  260.2 2.9 fusion.16
  263.0 55.1 %all-gather.15.cloned.1.call-done = bf16[1024,1408]{1,0:T(8,128)(2,1)} async-done(((bf16[128,1408]{1,0:T(8,128)(2,1)}), bf16[1024,1408]{1,0:T(8,128)(2,1)}) %all-gather.15.cloned.1.call-update) | async-done | bytes 2883600 | tf_op jit(solution)/shard_map/all_gather | solution.py:12
  318.1 60.3 %all-gather.17.cloned.1.call-done = bf16[1408,1024]{1,0:T(8,128)(2,1)} async-done(((bf16[1408,128]{1,0:T(8,128)(2,1)}), bf16[1408,1024]{1,0:T(8,128)(2,1)}) %all-gather.17.cloned.1.call-update) | async-done | bytes 2883600 | tf_op jit(solution)/shard_map/all_gather | solution.py:42
  378.4 5.4 %convolution_convert_fusion = bf16[256,1024]{1,0:T(8,128)(2,1)} fusion(bf16[1408,1024]{1,0:T(8,128)(2,1)} %all-gather.17.cloned.1.call-done, bf16[1024,1408]{1,0:T(8,128)(2,1)} %all-gather.15.cloned.1.call-done, f32[256,1408]{1,0:T(8,128)S(1)} %fusion.16, bf16[256,1024]{1,0:T(8,128)(2,1)S(1)} %all_gather.28, f32[1024]{0:T(1024)S(1)} %copy-done.2, ...), kind=kOutput, calls=%fused_computation.6 | convolution fusion | flops 1479868416 | bytes 8262656 | tf_op jit(solution)/shard_map/dot_general | solution.py:80
  383.8 6.3 %reduce-scatter.5.cloned.1.call-done = bf16[256,512]{1,0:T(8,128)(2,1)} async-done(((bf16[256,1024]{1,0:T(8,128)(2,1)}), bf16[256,512]{1,0:T(8,128)(2,1)}) %reduce-scatter.5.cloned.1.call-update) | async-done | bytes 262160 | tf_op jit(solution)/shard_map/reduce_scatter | solution.py:81
  390.1 1.1 fusion.7
  391.2 2.5 psum.7
  393.7 1.8 fusion.9
  (24 shorter events, 1.6 us)
Async XLA Ops:
  6.5 63.0 %all-gather.7.cloned.1.call-start = ((), (), s32[]{:S(2)}) async-start(), calls=%async_computation.2 | async-start | bytes 3244032 | tf_op jit(solution)/shard_map/all_gather | solution.py:12
  7.3 122.6 %all-gather.11.cloned.1.call-start = ((), (), s32[]{:S(2)}) async-start(), calls=%async_computation.4 | async-start | bytes 3244032 | tf_op jit(solution)/shard_map/all_gather | solution.py:42
  8.0 179.5 %all-gather.9.cloned.1.call-start = ((), (), s32[]{:S(2)}) async-start(), calls=%async_computation.3 | async-start | bytes 3244032 | tf_op jit(solution)/shard_map/all_gather | solution.py:12
  8.7 190.9 %reduce-scatter.3.cloned.1.call-start = ((), (), s32[]{:S(2)}) async-start(), calls=%async_computation.5 | async-start | bytes 786432 | tf_op jit(solution)/shard_map/reduce_scatter | solution.py:70
  72.4 127.3 %copy-start = (bf16[128,1024]{1,0:T(8,128)(2,1)S(1)}, bf16[128,1024]{1,0:T(8,128)(2,1)}, u32[]{:S(2)}) copy-start(bf16[128,1024]{1,0:T(8,128)(2,1)} %param.11) | copy-start | bytes 786436
  72.4 127.3 %copy-start.1 = (bf16[256,1024]{1,0:T(8,128)(2,1)S(1)}, bf16[256,1024]{1,0:T(8,128)(2,1)}, u32[]{:S(2)}) copy-start(bf16[256,1024]{1,0:T(8,128)(2,1)} %param.12) | copy-start | bytes 1572868
  192.9 67.2 %copy-start.2 = (f32[1024]{0:T(1024)S(1)}, f32[1024]{0:T(1024)}, u32[]{:S(2)}) copy-start(f32[1024]{0:T(1024)} %param.17) | copy-start | bytes 12292
  193.0 67.2 %all-gather.13.cloned.1.call-start = ((), (), s32[]{:S(2)}) async-start(), calls=%async_computation.6 | async-start | bytes 3244032 | tf_op jit(solution)/shard_map/all_gather | solution.py:12
  193.5 124.6 %all-gather.15.cloned.1.call-start = ((), (), s32[]{:S(2)}) async-start(), calls=%async_computation.7 | async-start | bytes 3244032 | tf_op jit(solution)/shard_map/all_gather | solution.py:12
  194.1 184.3 %all-gather.17.cloned.1.call-start = ((), (), s32[]{:S(2)}) async-start(), calls=%async_computation.8 | async-start | bytes 3244032 | tf_op jit(solution)/shard_map/all_gather | solution.py:42
  194.9 195.2 %reduce-scatter.5.cloned.1.call-start = ((), (), s32[]{:S(2)}) async-start(), calls=%async_computation.9 | async-start | bytes 786432 | tf_op jit(solution)/shard_map/reduce_scatter | solution.py:81
  263.0 130.7 %copy-start.3 = (f32[512]{0:T(512)S(1)}, f32[512]{0:T(512)}, u32[]{:S(2)}) copy-start(f32[512]{0:T(512)} %param.21) | copy-start | bytes 6148
Sparse Core Ops, SparseCore 0:
  9.5 60.0 all-gather.6
  71.6 58.1 all-gather.10
  132.0 55.4 all-gather.8
  193.1 6.5 reduce-scatter.2
  201.7 58.4 all-gather.12
  262.2 55.9 all-gather.14
  320.2 58.1 all-gather.16
  384.0 6.0 reduce-scatter.4
where the time goes:
time: 403 us; the launch traced here: 402 us
  waiting for transfers between devices  359 us (89%)
  matrix products  16.5 us (4%)
  between operations  13.6 us (3%)
  blocking collectives  6.95 us (2%)
  other arithmetic  6.36 us (2%)
    all_gather x4, waiting for transfers between devices, gathered(): return lax.all_gather(part, axis, axis=dim, tiled=True)  226 us
    all_gather x2, waiting for transfers between devices, outer_weight(): return lax.all_gather(w_down, 'fs', axis=1, tiled=True)  118 us
  transfers between devices with their start and end apart: 8, of which 8 were waited for; matrix products, arithmetic and copies ran while one was open for 2% of the time, Pallas kernels for 0%

commit v1 on v0

--- a/solution.py
+++ b/solution.py
@@ -4,6 +4,27 @@
 from jax.sharding import PartitionSpec as P
 
 EPS = 1e-06
+
+
+def collect(x, axis, dim):
+    size, here, extent = (lax.axis_size(axis), lax.axis_index(axis), x.shape[dim])
+    right = [(i, (i + 1) % size) for i in range(size)]
+    behind = [(i, (i - 1) % size) for i in range(size)]
+    out = jnp.zeros((*x.shape[:dim], size * extent, *x.shape[dim + 1 :]), x.dtype)
+    out = lax.dynamic_update_slice_in_dim(out, x, here * extent, axis=dim)
+    from_left = from_right = x
+    half = size // 2
+    for hop in range(1, half + 1):
+        from_left = lax.ppermute(from_left, axis, right)
+        out = lax.dynamic_update_slice_in_dim(
+            out, from_left, (here - hop) % size * extent, axis=dim
+        )
+        if hop < size - half:
+            from_right = lax.ppermute(from_right, axis, behind)
+            out = lax.dynamic_update_slice_in_dim(
+                out, from_right, (here + hop) % size * extent, axis=dim
+            )
+    return out
 
 
 def over_all(slab, axis, dim):
@@ -39,7 +60,7 @@
 
 
 def outer_weight(w_down):
-    return lax.all_gather(w_down, "fs", axis=1, tiled=True)
+    return collect(w_down, "fs", 1)
 
 
 def local(

time: 403 us -> 337 us (0.84)
  waiting for transfers between devices: 359 us -> 248 us
  starting transfers between devices: 0.27 us -> 36.8 us
  local copies, waits for them, and re-layouts: 0.02 us -> 6.58 us
    all_gather x2 -> x0, waiting for transfers between devices: 118 us -> none  [outer_weight(): return lax.all_gather(w_down, 'fs', axis=1, tiled=True)]
    ppermute x0 -> x14, waiting for transfers between devices: none -> 106 us  [the longest x8 83.6 us: collect(): from_left = lax.ppermute(from_left, axis, right)]
    all_gather x4, waiting for transfers between devices: 226 us -> 133 us  [gathered(): return lax.all_gather(part, axis, axis=dim, tiled=True)]
    ppermute x0 -> x14, starting transfers between devices: none -> 36.6 us  [the longest x6 23.8 us: collect(): from_right = lax.ppermute(from_right, axis, behind)]
    dynamic_update_slice x0 -> x16, local copies, waits for them, and re-layouts: none -> 5.85 us  [the longest x8 2.9 us: collect(): lax.dynamic_update_slice_in_dim(out, from_left, (here - hop) % size * ext...]
    reduce_scatter x1, waiting for transfers between devices: 4.74 us -> 0.02 us  [local(): lax.psum_scatter(row_terms().astype(jnp.bfloat16), 'tp', scatter_dimensio...]
  transfers between devices with their start and end apart: 8 -> 20, of which waited for: 8 -> 17; matrix products, arithmetic and copies ran while one was open for 2% -> 5% of each run, Pallas kernels for 0% -> 0%
where the time goes in v1:
time: 337 us; the launch traced here: 336 us
  waiting for transfers between devices  248 us (74%)
  starting transfers between devices  36.8 us (11%)
  matrix products  17.7 us (5%)
  between operations  13.7 us (4%)
  blocking collectives  6.83 us (2%)
  local copies, waits for them, and re-layouts  6.58 us (2%)
  other arithmetic  6.5 us (2%)
    all_gather x4, waiting for transfers between devices, gathered(): return lax.all_gather(part, axis, axis=dim, tiled=True)  133 us
    ppermute x8, waiting for transfers between devices, collect(): from_left = lax.ppermute(from_left, axis, right)  83.6 us
    ppermute x6, starting transfers between devices, collect(): from_right = lax.ppermute(from_right, axis, behind)  23.8 us
    ppermute x6, waiting for transfers between devices, collect(): from_right = lax.ppermute(from_right, axis, behind)  22.7 us
    ppermute x8, starting transfers between devices, collect(): from_left = lax.ppermute(from_left, axis, right)  12.8 us
    dot_general x2, matrix products, add_both(): jnp.dot(columns, pieces[0], preferred_element_type=jnp.float32)  7.89 us
  transfers between devices with their start and end apart: 20, of which 17 were waited for; matrix products, arithmetic and copies ran while one was open for 5% of the time, Pallas kernels for 0%

profile of v1, /device:TPU:0, one launch (start us, length us, event | category | flops | bytes accessed | tf_op | source)
XLA Modules:
  0.0 336.2 jit_solution(15648035602739374002)
XLA Ops:
  8.1 3.0 collective-permute-start
  11.1 3.1 collective-permute-start.1
  19.1 11.5 %collective-permute-done = bf16[1408,128]{1,0:T(8,128)(2,1)} collective-permute-done((bf16[1408,128]{1,0:T(8,128)(2,1)}, bf16[1408,128]{1,0:T(8,128)(2,1)}, u32[]{:S(2)}, u32[]{:S(2)}) %collective-permute-start) | collective-permute-done | bytes 360480 | tf_op jit(solution)/shard_map/ppermute | solution.py:18
  33.2 3.0 collective-permute-start.3
  38.4 10.2 %collective-permute-done.2 = bf16[1408,128]{1,0:T(8,128)(2,1)S(1)} collective-permute-done((bf16[1408,128]{1,0:T(8,128)(2,1)}, bf16[1408,128]{1,0:T(8,128)(2,1)S(1)}, u32[]{:S(2)}, u32[]{:S(2)}) %collective-permute-start.2) | collective-permute-done | bytes 360480 | tf_op jit(solution)/shard_map/ppermute | solution.py:18
  50.4 9.3 %collective-permute-start.5 = (bf16[1408,128]{1,0:T(8,128)(2,1)S(1)}, bf16[1408,128]{1,0:T(8,128)(2,1)S(1)}, u32[]{:S(2)}, u32[]{:S(2)}) collective-permute-start(bf16[1408,128]{1,0:T(8,128)(2,1)S(1)} %collective-permute-done.3), channel_id=1, source_target_pairs={{0,14},{2,0},{4,2},{6,4},{8,6},{10,8},{12,10},{14,12},{1,15},{3,1}... | collective-permute-start | bytes 1081352 | tf_op jit(solution)/shard_map/ppermute | solution.py:23
  60.0 13.2 %collective-permute-done.4 = bf16[1408,128]{1,0:T(8,128)(2,1)S(1)} collective-permute-done((bf16[1408,128]{1,0:T(8,128)(2,1)S(1)}, bf16[1408,128]{1,0:T(8,128)(2,1)S(1)}, u32[]{:S(2)}, u32[]{:S(2)}) %collective-permute-start.4) | collective-permute-done | bytes 360480 | tf_op jit(solution)/shard_map/ppermute | solution.py:18
  78.3 9.0 %collective-permute-done.6 = bf16[1408,128]{1,0:T(8,128)(2,1)S(1)} collective-permute-done((bf16[1408,128]{1,0:T(8,128)(2,1)S(1)}, bf16[1408,128]{1,0:T(8,128)(2,1)S(1)}, u32[]{:S(2)}, u32[]{:S(2)}) %collective-permute-start.6) | collective-permute-done | bytes 360480 | tf_op jit(solution)/shard_map/ppermute | solution.py:18
  87.4 13.1 %all-gather.5.cloned.1.call-done = bf16[1024,1408]{1,0:T(8,128)(2,1)} async-done(((bf16[128,1408]{1,0:T(8,128)(2,1)}), bf16[1024,1408]{1,0:T(8,128)(2,1)}) %all-gather.5.cloned.1.call-update) | async-done | bytes 2883600 | tf_op jit(solution)/shard_map/all_gather | solution.py:33
  100.5 3.9 %fusion.20 = f32[256,1408]{1,0:T(8,128)} fusion(bf16[256,1024]{1,0:T(8,128)(2,1)S(1)} %all_gather.18, bf16[1024,1408]{1,0:T(8,128)(2,1)} %all-gather.5.cloned.1.call-done), kind=kOutput, calls=%fused_computation.49 | convolution fusion | flops 738197504 | bytes 4849664 | tf_op jit(solution)/shard_map/dot_general | solution.py:53
  104.4 54.4 %all-gather.7.cloned.1.call-done = bf16[1024,1408]{1,0:T(8,128)(2,1)} async-done(((bf16[128,1408]{1,0:T(8,128)(2,1)}), bf16[1024,1408]{1,0:T(8,128)(2,1)}) %all-gather.7.cloned.1.call-update) | async-done | bytes 2883600 | tf_op jit(solution)/shard_map/all_gather | solution.py:33
  158.8 4.9 %convolution_convert_fusion.1 = bf16[256,1024]{1,0:T(8,128)(2,1)} fusion(bf16[1408,1024]{1,0:T(8,128)(2,1)S(1)} %constant_dynamic-update-slice_fusion.8, bf16[256,1024]{1,0:T(8,128)(2,1)S(1)} %all_gather.18, bf16[1024,1408]{1,0:T(8,128)(2,1)} %all-gather.7.cloned.1.call-done, f32[256,1408]{1,0:T(8,128)} %fusion.20), kind=kOutput, calls=%fused_computation.7 | convolution fusion | flops 1478819840 | bytes 8257536 | tf_op jit(solution)/shard_map/dot_general | solution.py:89
  165.5 4.2 %collective-permute-start.8 = (bf16[1408,128]{1,0:T(8,128)(2,1)}, bf16[1408,128]{1,0:T(8,128)(2,1)}, u32[]{:S(2)}, u32[]{:S(2)}) collective-permute-start(bf16[1408,128]{1,0:T(8,128)(2,1)} %param.20), channel_id=1, source_target_pairs={{0,14},{2,0},{4,2},{6,4},{8,6},{10,8},{12,10},{14,12},{1,15},{3,1}... | collective-permute-start | bytes 1081352 | tf_op jit(solution)/shard_map/ppermute | solution.py:23
  170.2 9.3 %collective-permute-done.7 = bf16[1408,128]{1,0:T(8,128)(2,1)} collective-permute-done((bf16[1408,128]{1,0:T(8,128)(2,1)}, bf16[1408,128]{1,0:T(8,128)(2,1)}, u32[]{:S(2)}, u32[]{:S(2)}) %collective-permute-start.7) | collective-permute-done | bytes 360480 | tf_op jit(solution)/shard_map/ppermute | solution.py:18
  187.1 10.7 %collective-permute-done.9 = bf16[1408,128]{1,0:T(8,128)(2,1)S(1)} collective-permute-done((bf16[1408,128]{1,0:T(8,128)(2,1)}, bf16[1408,128]{1,0:T(8,128)(2,1)S(1)}, u32[]{:S(2)}, u32[]{:S(2)}) %collective-permute-start.9) | collective-permute-done | bytes 360480 | tf_op jit(solution)/shard_map/ppermute | solution.py:18
  197.8 5.8 %collective-permute-done.10 = bf16[1408,128]{1,0:T(8,128)(2,1)S(1)} collective-permute-done((bf16[1408,128]{1,0:T(8,128)(2,1)}, bf16[1408,128]{1,0:T(8,128)(2,1)S(1)}, u32[]{:S(2)}, u32[]{:S(2)}) %collective-permute-start.10) | collective-permute-done | bytes 360480 | tf_op jit(solution)/shard_map/ppermute | solution.py:23
  206.0 10.5 %collective-permute-done.11 = bf16[1408,128]{1,0:T(8,128)(2,1)S(1)} collective-permute-done((bf16[1408,128]{1,0:T(8,128)(2,1)S(1)}, bf16[1408,128]{1,0:T(8,128)(2,1)S(1)}, u32[]{:S(2)}, u32[]{:S(2)}) %collective-permute-start.11) | collective-permute-done | bytes 360480 | tf_op jit(solution)/shard_map/ppermute | solution.py:18
  216.6 13.7 %collective-permute-done.12 = bf16[1408,128]{1,0:T(8,128)(2,1)S(1)} collective-permute-done((bf16[1408,128]{1,0:T(8,128)(2,1)S(1)}, bf16[1408,128]{1,0:T(8,128)(2,1)S(1)}, u32[]{:S(2)}, u32[]{:S(2)}) %collective-permute-start.12) | collective-permute-done | bytes 360480 | tf_op jit(solution)/shard_map/ppermute | solution.py:23
  230.4 9.1 %collective-permute-done.13 = bf16[1408,128]{1,0:T(8,128)(2,1)S(1)} collective-permute-done((bf16[1408,128]{1,0:T(8,128)(2,1)S(1)}, bf16[1408,128]{1,0:T(8,128)(2,1)S(1)}, u32[]{:S(2)}, u32[]{:S(2)}) %collective-permute-start.13) | collective-permute-done | bytes 360480 | tf_op jit(solution)/shard_map/ppermute | solution.py:18
  243.2 10.5 %all-gather.9.cloned.1.call-done = bf16[1024,1408]{1,0:T(8,128)(2,1)} async-done(((bf16[128,1408]{1,0:T(8,128)(2,1)}), bf16[1024,1408]{1,0:T(8,128)(2,1)}) %all-gather.9.cloned.1.call-update) | async-done | bytes 2883600 | tf_op jit(solution)/shard_map/all_gather | solution.py:33
  253.7 4.0 %fusion.16 = f32[256,1408]{1,0:T(8,128)} fusion(bf16[1024,1408]{1,0:T(8,128)(2,1)} %all-gather.9.cloned.1.call-done, bf16[256,1024]{1,0:T(8,128)(2,1)S(1)} %all_gather.21, f32[1024]{0:T(1024)S(1)} %copy-done.3, f32[256]{0:T(256)S(1)} %add_rsqrt_fusion.1), kind=kOutput, calls=%fused_computation.27 | convolution fusion | flops 739246080 | bytes 4854784 | tf_op jit(solution)/shard_map/dot_general | solution.py:53
  257.7 54.6 %all-gather.11.cloned.1.call-done = bf16[1024,1408]{1,0:T(8,128)(2,1)} async-done(((bf16[128,1408]{1,0:T(8,128)(2,1)}), bf16[1024,1408]{1,0:T(8,128)(2,1)}) %all-gather.11.cloned.1.call-update) | async-done | bytes 2883600 | tf_op jit(solution)/shard_map/all_gather | solution.py:33
  312.3 5.0 %convolution_convert_fusion = bf16[256,1024]{1,0:T(8,128)(2,1)} fusion(bf16[1408,1024]{1,0:T(8,128)(2,1)S(1)} %constant_dynamic-update-slice_fusion, bf16[1024,1408]{1,0:T(8,128)(2,1)} %all-gather.11.cloned.1.call-done, f32[256,1408]{1,0:T(8,128)} %fusion.16, bf16[256,1024]{1,0:T(8,128)(2,1)S(1)} %all_gather.21, f32[1024]{0:T(1024)S(1)} %copy-done.3, ...), kind=kOutput, calls=%fused_computation.6 | convolution fusion | flops 1479868416 | bytes 8262656 | tf_op jit(solution)/shard_map/dot_general | solution.py:101
  317.3 6.7 %reduce-scatter.5.cloned.1.call-done = bf16[256,512]{1,0:T(8,128)(2,1)} async-done(((bf16[256,1024]{1,0:T(8,128)(2,1)}), bf16[256,512]{1,0:T(8,128)(2,1)}) %reduce-scatter.5.cloned.1.call-update) | async-done | bytes 262160 | tf_op jit(solution)/shard_map/reduce_scatter | solution.py:102
  (66 shorter events, 39.7 us)
Async XLA Ops:
  6.5 94.0 %all-gather.5.cloned.1.call-start = ((), (), s32[]{:S(2)}) async-start(), calls=%async_computation.2 | async-start | bytes 3244032 | tf_op jit(solution)/shard_map/all_gather | solution.py:33
  7.3 151.6 %all-gather.7.cloned.1.call-start = ((), (), s32[]{:S(2)}) async-start(), calls=%async_computation.3 | async-start | bytes 3244032 | tf_op jit(solution)/shard_map/all_gather | solution.py:33
  8.0 231.7 %reduce-scatter.3.cloned.1.call-start = ((), (), s32[]{:S(2)}) async-start(), calls=%async_computation.4 | async-start | bytes 786432 | tf_op jit(solution)/shard_map/reduce_scatter | solution.py:91
  8.1 22.6 %collective-permute-start = (bf16[1408,128]{1,0:T(8,128)(2,1)}, bf16[1408,128]{1,0:T(8,128)(2,1)}, u32[]{:S(2)}, u32[]{:S(2)}) collective-permute-start(bf16[1408,128]{1,0:T(8,128)(2,1)} %param.16), channel_id=1, source_target_pairs={{0,2},{2,4},{4,6},{6,8},{8,10},{10,12},{12,14},{14,0},{1,3},{3,5},... | collective-permute-start | bytes 1081352 | tf_op jit(solution)/shard_map/ppermute | solution.py:18
  11.1 22.1 %collective-permute-start.1 = (bf16[1408,128]{1,0:T(8,128)(2,1)}, bf16[1408,128]{1,0:T(8,128)(2,1)}, u32[]{:S(2)}, u32[]{:S(2)}) collective-permute-start(bf16[1408,128]{1,0:T(8,128)(2,1)} %param.16), channel_id=1, source_target_pairs={{0,14},{2,0},{4,2},{6,4},{8,6},{10,8},{12,10},{14,12},{1,15},{3,1}... | collective-permute-start | bytes 1081352 | tf_op jit(solution)/shard_map/ppermute | solution.py:23
  30.7 18.0 %collective-permute-start.2 = (bf16[1408,128]{1,0:T(8,128)(2,1)}, bf16[1408,128]{1,0:T(8,128)(2,1)S(1)}, u32[]{:S(2)}, u32[]{:S(2)}) collective-permute-start(bf16[1408,128]{1,0:T(8,128)(2,1)} %collective-permute-done), channel_id=1, source_target_pairs={{0,2},{2,4},{4,6},{6,8},{8,10},{10,12},{12,14},{14,0},{1,3},{3,5},... | collective-permute-start | bytes 1081352 | tf_op jit(solution)/shard_map/ppermute | solution.py:18
  33.2 17.2 %collective-permute-start.3 = (bf16[1408,128]{1,0:T(8,128)(2,1)}, bf16[1408,128]{1,0:T(8,128)(2,1)S(1)}, u32[]{:S(2)}, u32[]{:S(2)}) collective-permute-start(bf16[1408,128]{1,0:T(8,128)(2,1)} %collective-permute-done.1), channel_id=1, source_target_pairs={{0,14},{2,0},{4,2},{6,4},{8,6},{10,8},{12,10},{14,12},{1,15},{3,1}... | collective-permute-start | bytes 1081352 | tf_op jit(solution)/shard_map/ppermute | solution.py:23
  48.7 24.5 %collective-permute-start.4 = (bf16[1408,128]{1,0:T(8,128)(2,1)S(1)}, bf16[1408,128]{1,0:T(8,128)(2,1)S(1)}, u32[]{:S(2)}, u32[]{:S(2)}) collective-permute-start(bf16[1408,128]{1,0:T(8,128)(2,1)S(1)} %collective-permute-done.2), channel_id=1, source_target_pairs={{0,2},{2,4},{4,6},{6,8},{8,10},{10,12},{12,14},{14,0},{1,3},{3,5},... | collective-permute-start | bytes 1081352 | tf_op jit(solution)/shard_map/ppermute | solution.py:18
  50.4 27.7 %collective-permute-start.5 = (bf16[1408,128]{1,0:T(8,128)(2,1)S(1)}, bf16[1408,128]{1,0:T(8,128)(2,1)S(1)}, u32[]{:S(2)}, u32[]{:S(2)}) collective-permute-start(bf16[1408,128]{1,0:T(8,128)(2,1)S(1)} %collective-permute-done.3), channel_id=1, source_target_pairs={{0,14},{2,0},{4,2},{6,4},{8,6},{10,8},{12,10},{14,12},{1,15},{3,1}... | collective-permute-start | bytes 1081352 | tf_op jit(solution)/shard_map/ppermute | solution.py:23
  73.2 14.1 %collective-permute-start.6 = (bf16[1408,128]{1,0:T(8,128)(2,1)S(1)}, bf16[1408,128]{1,0:T(8,128)(2,1)S(1)}, u32[]{:S(2)}, u32[]{:S(2)}) collective-permute-start(bf16[1408,128]{1,0:T(8,128)(2,1)S(1)} %collective-permute-done.4), channel_id=1, source_target_pairs={{0,2},{2,4},{4,6},{6,8},{8,10},{10,12},{12,14},{14,0},{1,3},{3,5},... | collective-permute-start | bytes 1081352 | tf_op jit(solution)/shard_map/ppermute | solution.py:18
  163.7 6.4 %copy-start.2 = (bf16[1408,128]{1,0:T(8,128)(2,1)S(1)}, bf16[1408,128]{1,0:T(8,128)(2,1)}, u32[]{:S(2)}) copy-start(bf16[1408,128]{1,0:T(8,128)(2,1)} %param.20) | copy-start | bytes 1081348
  163.7 90.0 %all-gather.9.cloned.1.call-start = ((), (), s32[]{:S(2)}) async-start(), calls=%async_computation.5 | async-start | bytes 3244032 | tf_op jit(solution)/shard_map/all_gather | solution.py:33
  164.3 148.0 %all-gather.11.cloned.1.call-start = ((), (), s32[]{:S(2)}) async-start(), calls=%async_computation.6 | async-start | bytes 3244032 | tf_op jit(solution)/shard_map/all_gather | solution.py:33
  164.9 159.1 %reduce-scatter.5.cloned.1.call-start = ((), (), s32[]{:S(2)}) async-start(), calls=%async_computation.7 | async-start | bytes 786432 | tf_op jit(solution)/shard_map/reduce_scatter | solution.py:102
  164.9 14.6 %collective-permute-start.7 = (bf16[1408,128]{1,0:T(8,128)(2,1)}, bf16[1408,128]{1,0:T(8,128)(2,1)}, u32[]{:S(2)}, u32[]{:S(2)}) collective-permute-start(bf16[1408,128]{1,0:T(8,128)(2,1)} %param.20), channel_id=1, source_target_pairs={{0,2},{2,4},{4,6},{6,8},{8,10},{10,12},{12,14},{14,0},{1,3},{3,5},... | collective-permute-start | bytes 1081352 | tf_op jit(solution)/shard_map/ppermute | solution.py:18
  165.5 17.4 %collective-permute-start.8 = (bf16[1408,128]{1,0:T(8,128)(2,1)}, bf16[1408,128]{1,0:T(8,128)(2,1)}, u32[]{:S(2)}, u32[]{:S(2)}) collective-permute-start(bf16[1408,128]{1,0:T(8,128)(2,1)} %param.20), channel_id=1, source_target_pairs={{0,14},{2,0},{4,2},{6,4},{8,6},{10,8},{12,10},{14,12},{1,15},{3,1}... | collective-permute-start | bytes 1081352 | tf_op jit(solution)/shard_map/ppermute | solution.py:23
  170.1 69.6 %copy-start = (bf16[128,1024]{1,0:T(8,128)(2,1)S(1)}, bf16[128,1024]{1,0:T(8,128)(2,1)}, u32[]{:S(2)}) copy-start(bf16[128,1024]{1,0:T(8,128)(2,1)} %param.11) | copy-start | bytes 786436
  179.6 18.2 %collective-permute-start.9 = (bf16[1408,128]{1,0:T(8,128)(2,1)}, bf16[1408,128]{1,0:T(8,128)(2,1)S(1)}, u32[]{:S(2)}, u32[]{:S(2)}) collective-permute-start(bf16[1408,128]{1,0:T(8,128)(2,1)} %collective-permute-done.7), channel_id=1, source_target_pairs={{0,2},{2,4},{4,6},{6,8},{8,10},{10,12},{12,14},{14,0},{1,3},{3,5},... | collective-permute-start | bytes 1081352 | tf_op jit(solution)/shard_map/ppermute | solution.py:18
  182.9 20.7 %collective-permute-start.10 = (bf16[1408,128]{1,0:T(8,128)(2,1)}, bf16[1408,128]{1,0:T(8,128)(2,1)S(1)}, u32[]{:S(2)}, u32[]{:S(2)}) collective-permute-start(bf16[1408,128]{1,0:T(8,128)(2,1)} %collective-permute-done.8), channel_id=1, source_target_pairs={{0,14},{2,0},{4,2},{6,4},{8,6},{10,8},{12,10},{14,12},{1,15},{3,1}... | collective-permute-start | bytes 1081352 | tf_op jit(solution)/shard_map/ppermute | solution.py:23
  187.1 66.6 %copy-start.3 = (f32[1024]{0:T(1024)S(1)}, f32[1024]{0:T(1024)}, u32[]{:S(2)}) copy-start(f32[1024]{0:T(1024)} %param.17) | copy-start | bytes 12292
  197.8 18.7 %collective-permute-start.11 = (bf16[1408,128]{1,0:T(8,128)(2,1)S(1)}, bf16[1408,128]{1,0:T(8,128)(2,1)S(1)}, u32[]{:S(2)}, u32[]{:S(2)}) collective-permute-start(bf16[1408,128]{1,0:T(8,128)(2,1)S(1)} %collective-permute-done.9), channel_id=1, source_target_pairs={{0,2},{2,4},{4,6},{6,8},{8,10},{10,12},{12,14},{14,0},{1,3},{3,5},... | collective-permute-start | bytes 1081352 | tf_op jit(solution)/shard_map/ppermute | solution.py:18
  203.6 26.7 %collective-permute-start.12 = (bf16[1408,128]{1,0:T(8,128)(2,1)S(1)}, bf16[1408,128]{1,0:T(8,128)(2,1)S(1)}, u32[]{:S(2)}, u32[]{:S(2)}) collective-permute-start(bf16[1408,128]{1,0:T(8,128)(2,1)S(1)} %collective-permute-done.10), channel_id=1, source_target_pairs={{0,14},{2,0},{4,2},{6,4},{8,6},{10,8},{12,10},{14,12},{1,15},{3,1}... | collective-permute-start | bytes 1081352 | tf_op jit(solution)/shard_map/ppermute | solution.py:23
  216.5 23.1 %collective-permute-start.13 = (bf16[1408,128]{1,0:T(8,128)(2,1)S(1)}, bf16[1408,128]{1,0:T(8,128)(2,1)S(1)}, u32[]{:S(2)}, u32[]{:S(2)}) collective-permute-start(bf16[1408,128]{1,0:T(8,128)(2,1)S(1)} %collective-permute-done.11), channel_id=1, source_target_pairs={{0,2},{2,4},{4,6},{6,8},{8,10},{10,12},{12,14},{14,0},{1,3},{3,5},... | collective-permute-start | bytes 1081352 | tf_op jit(solution)/shard_map/ppermute | solution.py:18
  257.7 69.9 %copy-start.4 = (f32[512]{0:T(512)S(1)}, f32[512]{0:T(512)}, u32[]{:S(2)}) copy-start(f32[512]{0:T(512)} %param.21) | copy-start | bytes 6148
  (1 other events, 4.8 us)
Sparse Core Ops, SparseCore 0:
  9.5 90.9 all-gather.4
  102.7 56.0 all-gather.6
  163.8 6.5 reduce-scatter.2
  172.5 81.2 all-gather.8
  255.8 56.5 all-gather.10
  317.4 6.5 reduce-scatter.4
